TPU v7x, 128 devices: a whole 4x4x4 slice. The times are simulated.
128 devices in a mesh: sp: 16 (over z, x), tp: 8 (over y, core).
Axes of the slice: x: 4, y: 4, z: 4, core: 2. Of those that a mesh axis runs over, the one named last changes fastest.
Arguments:
- x_in: bfloat16 [16, 6144, 2048], P('tp', 'sp'), may hold values from -13 to 13
- x_new: bfloat16 [16, 2048], P('sp'), may hold values from -6 to 6
- w_x: bfloat16 [2048, 2048], replicated, may hold values from -0.125 to 0.125
- w_b: bfloat16 [2048, 1024], replicated, may hold values from -0.125 to 0.125
- w_c: bfloat16 [2048, 1024], replicated, may hold values from -0.125 to 0.125
- w_dt: bfloat16 [2048, 32], replicated, may hold values from -0.125 to 0.125
- w_z: bfloat16 [2048, 2048], P(None, 'tp'), may hold values from -3 to 3
- conv_w: float32 [4, 4096], replicated, may hold values from -3 to 3
- conv_b: float32 [4096], replicated, may hold values from -3 to 3
- dt_bias: float32 [32], replicated, may hold values from -4 to -2
- a_log: float32 [32], replicated, may hold values from -12 to 0
- d_skip: float32 [32], replicated, may hold values from 1 to 8
- norm_g: float32 [32, 64], P('tp'), may hold values from 0.1 to 1.9
Outputs:
- state_cache: bfloat16 [16, 32, 64, 128], P('sp', 'tp')
- read_out: bfloat16 [16, 32, 64], P('sp', 'tp')
All inputs are finite; a program needn't handle non-finite values.
Results may differ from a plain program's by a relative error of at most 0.015.
Values may be sent and summed in bfloat16 or wider, within the bound.
A program may use at most 128 MiB of HBM per device.

v0:
```python
import jax
import jax.numpy as jnp
from jax import lax
from jax.sharding import Mesh
from jax.sharding import PartitionSpec as P

H = 32
P_SIZE = 64
G = 8
N = 128
KW = 4
R = 4
TP = ("tp_0", "tp_1")
eps = 1e-05


def copy_for_each(value, axis):
    copies = jnp.broadcast_to(value, (lax.axis_size(axis), *value.shape))
    return lax.all_to_all(copies, axis, split_axis=0, concat_axis=0, tiled=True)


def combined_pairwise(pieces, combine):
    while len(jax.tree.leaves(pieces)[0]) > 1:
        pieces = jax.vmap(combine)(*(pieces[side::2] for side in (0, 1)))
    return pieces[0]


def prefix(value, axis, combine, identity):
    devices, index = (lax.axis_size(axis), lax.axis_index(axis))
    passed = jnp.arange(devices) > index

    def kept(part, zero, own):
        part = jnp.where(
            passed.reshape(-1, *(1 for _ in own.shape)), part, jnp.asarray(zero, own.dtype)
        )
        return part[::-1]

    pieces = copy_for_each(value, axis)
    return combined_pairwise(kept(pieces, identity, value), combine)


def passed_along(value, axis, steps):
    count = lax.axis_size(axis)
    first, last = (max(0, -steps), min(count, count - steps))
    return lax.ppermute(value, axis, [(source, source + steps) for source in range(first, last)])


def broadcast(value, axis, root):
    return lax.dynamic_index_in_dim(lax.all_gather(value, axis), root, 0, keepdims=False)


def joined_along(pieces, dim):
    pieces = jnp.moveaxis(pieces, 0, dim)
    dims = pieces.shape
    return pieces.reshape(*dims[:dim], dims[dim] * dims[dim + 1], *dims[dim + 2 :])


def all_blocks(value, axes, sequence):
    pieces = value[None]
    for k in sequence:
        pieces = lax.all_gather(pieces, axes[k], axis=0, tiled=True)
    held = [lax.axis_size(axes[k]) for k in reversed(sequence)]
    pieces = pieces.reshape(*held, *value.shape)
    turned = sorted(range(len(sequence)), key=lambda place: sequence[len(sequence) - 1 - place])
    return pieces.transpose(*turned, *range(len(sequence), pieces.ndim)).reshape(-1, *value.shape)


def gather_axes(value, axes, sequence, dim):
    return joined_along(all_blocks(value, axes, sequence), dim)


def in_blocks(value, dim, devices):
    before, after = (value.shape[:dim], value.shape[dim + 1 :])
    return jnp.moveaxis(value.reshape(*before, devices, -1, *after), dim, 0)


def summed_on_arrival(value, axis, dim):
    devices = lax.axis_size(axis)
    pieces = lax.all_to_all(in_blocks(value, dim, devices), axis, 0, 0, tiled=True)
    return jnp.sum(pieces.astype(jnp.float32), axis=0)


def shift_conv(padded, weights, biases, col_count):
    acc_sum = biases + jnp.zeros(padded.shape[:1] + (col_count,) + padded.shape[2:], jnp.float32)
    for offset in range(KW):
        acc_sum = acc_sum + weights[offset] * padded[:, offset : offset + col_count].astype(
            jnp.float32
        )
    return jax.nn.silu(acc_sum).astype(jnp.bfloat16)


def project(token_rows, weight):
    flat_rows = token_rows.reshape(-1, token_rows.shape[-1])
    result = jnp.dot(flat_rows, weight, preferred_element_type=jnp.float32).astype(jnp.bfloat16)
    return result.reshape(token_rows.shape[:-1] + (weight.shape[1],))


def add_totals(earlier, later_part):
    return earlier + later_part


def decayed(step_sizes, rates, values, head_count):
    rest_sum = lax.cumsum(step_sizes, axis=1, reverse=True) - step_sizes
    totals = jnp.sum(step_sizes, axis=1)
    later_sum = prefix(totals, "sp", add_totals, jnp.zeros_like(totals))
    weight = jnp.exp(rates * (rest_sum + later_sum[:, None, :])) * step_sizes
    shaped = values.astype(jnp.float32).reshape(
        values.shape[0], values.shape[1], head_count, P_SIZE
    )
    return (weight[..., None] * shaped).astype(jnp.bfloat16)


def per_device(
    x_in, x_new, w_x, w_b, w_c, w_dt, w_z, conv_w, conv_b, dt_bias, a_log, d_skip, norm_g
):
    seq_count = x_in.shape[0]
    span_len = x_in.shape[1]
    tp_size = lax.axis_size(TP)
    sp_size = lax.axis_size("sp")
    tp_rank = lax.axis_index(TP)
    sp_rank = lax.axis_index("sp")
    heads_local = H // tp_size
    groups_local = G // tp_size
    inner_cols = H * P_SIZE
    state_cols = G * N
    edge_rows = KW - 1
    decay_rates = -jnp.exp(a_log)
    bias_local = lax.dynamic_slice_in_dim(dt_bias, tp_rank * heads_local, heads_local)
    rate_local = lax.dynamic_slice_in_dim(decay_rates, tp_rank * heads_local, heads_local)
    pre_values = project(x_in, w_x)
    pre_keys = project(x_in, w_b)
    raw_steps = project(x_in, w_dt)
    pre_query = project(x_in[:, span_len - edge_rows :], w_c)
    joined = jnp.concatenate([pre_values, pre_keys], axis=2)
    before = passed_along(joined[:, span_len - edge_rows :], "sp", 1)
    conved = shift_conv(
        jnp.concatenate([before, joined], axis=1),
        conv_w[:, : inner_cols + state_cols],
        conv_b[: inner_cols + state_cols],
        span_len,
    )
    tail_rows = jnp.concatenate([joined[:, span_len - edge_rows :], pre_query], axis=2)
    last_rows = broadcast(tail_rows, "sp", sp_size - 1)
    all_tails = gather_axes(last_rows, ("tp_0", "tp_1"), (0, 1), 0)
    step_sizes = jax.nn.softplus(raw_steps.astype(jnp.float32) + dt_bias)
    scaled = decayed(step_sizes, decay_rates, conved[..., :inner_cols], H)
    key_rows = conved[..., inner_cols:].reshape(seq_count, span_len, G, N)
    term_full = jnp.einsum(
        "slgrp,slgn->sgrpn",
        scaled.reshape(seq_count, span_len, G, R, P_SIZE),
        key_rows,
        preferred_element_type=jnp.float32,
    ).reshape(seq_count, H, P_SIZE, N)
    term_rows = lax.all_to_all(
        term_full.astype(jnp.bfloat16), TP, split_axis=1, concat_axis=0, tiled=True
    ).astype(term_full.dtype)
    state_piece = summed_on_arrival(term_rows.astype(jnp.bfloat16), "sp", 0)
    state_cache = state_piece.astype(jnp.bfloat16)
    seq_local = state_piece.shape[0]
    tails_local = lax.dynamic_slice_in_dim(all_tails, sp_rank * seq_local, seq_local, 0)
    value_cols = tp_rank * heads_local * P_SIZE
    group_cols = tp_rank * groups_local * N
    new_values = jnp.dot(
        x_new,
        lax.dynamic_slice_in_dim(w_x, value_cols, heads_local * P_SIZE, 1),
        preferred_element_type=jnp.float32,
    ).astype(jnp.bfloat16)
    new_keys = jnp.dot(
        x_new,
        lax.dynamic_slice_in_dim(w_b, group_cols, groups_local * N, 1),
        preferred_element_type=jnp.float32,
    ).astype(jnp.bfloat16)
    new_query = jnp.dot(
        x_new,
        lax.dynamic_slice_in_dim(w_c, group_cols, groups_local * N, 1),
        preferred_element_type=jnp.float32,
    ).astype(jnp.bfloat16)
    new_raw = jnp.dot(
        x_new,
        lax.dynamic_slice_in_dim(w_dt, tp_rank * heads_local, heads_local, 1),
        preferred_element_type=jnp.float32,
    ).astype(jnp.bfloat16)
    gate_new = jnp.dot(x_new, w_z, preferred_element_type=jnp.float32).astype(jnp.bfloat16)

    def new_conv(newest, col_start, col_count):
        history = lax.dynamic_slice_in_dim(tails_local, col_start, col_count, 2)
        padded = jnp.concatenate([history, newest[:, None, :]], axis=1)
        return shift_conv(
            padded,
            lax.dynamic_slice_in_dim(conv_w, col_start, col_count, 1),
            lax.dynamic_slice_in_dim(conv_b, col_start, col_count, 0),
            1,
        )[:, 0]

    conv_values = new_conv(new_values, value_cols, heads_local * P_SIZE)
    value_rows = conv_values.astype(jnp.float32).reshape(seq_local, groups_local, R, P_SIZE)
    conv_keys = new_conv(new_keys, inner_cols + group_cols, groups_local * N)
    conv_keys = conv_keys.astype(jnp.float32).reshape(seq_local, groups_local, N)
    conv_query = new_conv(new_query, inner_cols + state_cols + group_cols, groups_local * N)
    conv_query = conv_query.astype(jnp.float32).reshape(seq_local, groups_local, N)
    new_steps = jax.nn.softplus(new_raw.astype(jnp.float32) + bias_local)
    decay_new = jnp.exp(rate_local * new_steps).reshape(seq_local, groups_local, R)
    held_read = jnp.einsum(
        "sgrpn,sgn->sgrp", state_piece.reshape(seq_local, groups_local, R, P_SIZE, N), conv_query
    )
    inner_prod = jnp.sum(conv_query * conv_keys, axis=-1)
    step_group = new_steps.reshape(seq_local, groups_local, R)
    skip_local = lax.dynamic_slice_in_dim(d_skip, tp_rank * heads_local, heads_local).reshape(
        groups_local, R
    )
    output = (
        decay_new[..., None] * held_read
        + (step_group * inner_prod[:, :, None])[..., None] * value_rows
        + skip_local[None, :, :, None] * value_rows
    )
    gate_rows = gate_new.astype(jnp.float32).reshape(seq_local, groups_local, R, P_SIZE)
    gated_out = output * jax.nn.silu(gate_rows)
    group_ms = jnp.mean(gated_out * gated_out, axis=(2, 3))
    read_out = (
        gated_out
        * lax.rsqrt(group_ms + eps)[:, :, None, None]
        * norm_g.reshape(groups_local, R, P_SIZE)
    )
    read_out = read_out.astype(jnp.bfloat16).reshape(seq_local, heads_local, P_SIZE)
    return (state_cache, read_out)


def solution(mesh):
    finer = Mesh(mesh.devices.reshape(mesh.shape["sp"], 4, 2), ("sp", "tp_0", "tp_1"))
    return jax.shard_map(
        per_device,
        mesh=finer,
        in_specs=(
            P(TP, "sp", None),
            P("sp", None),
            P(),
            P(),
            P(),
            P(),
            P(None, TP),
            P(),
            P(),
            P(),
            P(),
            P(),
            P(TP, None),
        ),
        out_specs=(P("sp", TP, None, None), P("sp", TP, None)),
        check_vma=False,
    )
```

profile of v0, /device:TPU:0, one launch (start us, length us, event | category | flops | bytes accessed | tf_op | source)
XLA Modules:
  0.0 158.0 jit_solution(8769843090585375116)
XLA Ops:
  0.6 0.0 copy-start
  0.6 0.0 copy-start.10
  0.7 3.0 %fusion.8 = f32[768,32]{0,1:T(8,128)S(1)} fusion(bf16[768,2048]{1,0:T(8,128)(2,1)} %bitcast.261, bf16[2048,32]{0,1:T(8,128)(2,1)} %param.18), kind=kOutput, calls=%fused_computation.16 | convolution fusion | flops 100712448 | bytes 3375104 | tf_op jit(solution)/shard_map/dot_general | solution.py:94
  3.7 0.0 copy-done.10
  3.7 0.2 fusion.77
  3.9 0.6 broadcast_in_dim.21
  4.5 8.0 %all-to-all-start = ((f32[16,2,32]{2,1,0:T(2,128)}), f32[16,2,32]{2,1,0:T(2,128)S(1)}, u32[]{:S(2)}, u32[]{:S(2)}) async-start(f32[16,2,32]{2,1,0:T(2,128)} %broadcast_in_dim.21), calls=%async_computation | async-start | bytes 32768 | tf_op jit(solution)/shard_map/all_to_all | solution.py:19
  12.5 7.7 %convolution_convert_fusion.1 = bf16[768,1024]{1,0:T(8,128)(2,1)} fusion(bf16[768,2048]{1,0:T(8,128)(2,1)} %bitcast.262, bf16[2048,1024]{1,0:T(8,128)(2,1)} %param.16), kind=kOutput, calls=%fused_computation.12 | convolution fusion | flops 3222011904 | bytes 8912896 | tf_op jit(solution)/shard_map/dot_general | solution.py:94
  20.2 1.9 %copy.66 = bf16[2,384,1024]{1,2,0:T(8,128)(2,1)S(1)} copy(bf16[2,384,1024]{2,1,0:T(8,128)(2,1)} %bitcast.267) | data formatting | bytes 3145728 | tf_op jit(solution)/shard_map/reshape | solution.py:95
  22.1 11.9 %convolution_convert_fusion = bf16[768,2048]{1,0:T(8,128)(2,1)} fusion(bf16[768,2048]{1,0:T(8,128)(2,1)} %bitcast.263, bf16[2048,2048]{1,0:T(8,128)(2,1)} %param.15), kind=kOutput, calls=%fused_computation.7 | convolution fusion | flops 6444023808 | bytes 14680064 | tf_op jit(solution)/shard_map/dot_general | solution.py:94
  34.0 4.6 %copy.65 = bf16[2,384,2048]{1,2,0:T(8,128)(2,1)} copy(bf16[2,384,2048]{2,1,0:T(8,128)(2,1)} %bitcast.265) | data formatting | bytes 6291456 | tf_op jit(solution)/shard_map/reshape | solution.py:95
  38.6 2.9 %fusion.4 = bf16[2,3,3072]{1,2,0:T(8,128)(2,1)} fusion(bf16[2,384,2048]{1,2,0:T(8,128)(2,1)} %copy.65, bf16[2,384,1024]{1,2,0:T(8,128)(2,1)S(1)} %copy.66), kind=kLoop, calls=%fused_computation.13 | loop fusion | flops 73728 | bytes 4755456 | tf_op jit(solution)/shard_map/concatenate | solution.py:134
  41.6 2.4 %copy.67 = bf16[2,3,3072]{2,0,1:T(2,128)(2,1)} copy(bf16[2,3,3072]{1,2,0:T(8,128)(2,1)} %fusion.4) | data formatting | bytes 73728 | tf_op jit(solution)/shard_map/slice | solution.py:135
  43.9 4.0 %collective-permute-start = (bf16[2,3,3072]{2,0,1:T(2,128)(2,1)}, bf16[2,3,3072]{2,0,1:T(2,128)(2,1)S(1)}, u32[]{:S(2)}, u32[]{:S(2)}) collective-permute-start(bf16[2,3,3072]{2,0,1:T(2,128)(2,1)} %copy.67), channel_id=1, source_target_pairs={{0,8},{8,16},{16,24},{24,32},{32,40},{40,48},{48,56},{56,64},{64,7... | collective-permute-start | bytes 110600 | tf_op jit(solution)/shard_map/ppermute | solution.py:45
  47.9 0.9 slice.168
  48.8 0.6 exponential_negate_fusion
  49.5 0.0 copy-start.4
  49.5 2.8 %convolution_convert_fusion.3 = bf16[6,1024]{1,0:T(8,128)(2,1)S(1)} fusion(bf16[6,2048]{1,0:T(8,128)(2,1)S(1)} %reshape.243, bf16[2048,1024]{1,0:T(8,128)(2,1)} %param.17), kind=kOutput, calls=%fused_computation.17 | convolution fusion | flops 25171968 | bytes 4231168 | tf_op jit(solution)/shard_map/dot_general | solution.py:94
  52.4 7.5 %reduce-window.6 = f32[2,32,3,128]{3,1,2,0:T(8,128)S(1)} reduce-window(f32[2,32,3,128]{3,1,2,0:T(8,128)S(1)} %bitcast.276, f32[]{:T(128)} %constant.97.clone.1), window={size=1x1x1x128 pad=0_0x0_0x0_0x0_127}, to_apply=%region_0.1 | reduce-window | flops 3121152 | bytes 196612 | tf_op jit(solution)/shard_map/reduce-window
  59.9 0.1 copy.62
  60.0 0.3 copy.74
  60.3 3.2 %pad_maximum_fusion.1 = bf16[2,3,4096]{1,2,0:T(8,128)(2,1)} fusion(bf16[2,3,1024]{1,2,0:T(8,128)(2,1)S(1)} %copy.74, bf16[2,3,3072]{1,2,0:T(8,128)(2,1)} %fusion.4), kind=kLoop, calls=%fused_computation.10 | loop fusion | flops 98304 | bytes 98304 | tf_op jit(solution)/shard_map/concatenate | solution.py:142
  63.5 0.8 fusion.32
  64.3 0.0 copy-done.6
  64.3 0.6 dynamic_slice.68
  64.9 0.7 dynamic-slice.6
  65.6 0.0 all-to-all-done
  65.6 0.1 broadcast_select_fusion
  65.8 0.8 fusion.30
  66.6 0.0 collective-permute-done
  66.7 1.6 %copy.68 = bf16[2,3,3072]{1,2,0:T(8,128)(2,1)} copy(bf16[2,3,3072]{2,0,1:T(2,128)(2,1)S(1)} %collective-permute-done) | data formatting | bytes 73728 | tf_op jit(solution)/shard_map/ppermute | solution.py:45
  68.3 8.2 %maximum_maximum_fusion = bf16[2,387,3072]{1,2,0:T(8,128)(2,1)S(1)} fusion(bf16[2,384,1024]{1,2,0:T(8,128)(2,1)S(1)} %copy.66, bf16[2,384,2048]{1,2,0:T(8,128)(2,1)} %copy.65, bf16[2,3,3072]{1,2,0:T(8,128)(2,1)} %copy.68), kind=kLoop, calls=%fused_computation.1 | loop fusion | flops 14266368 | bytes 9510912 | tf_op jit(solution)/shard_map/concatenate | solution.py:137
  76.5 10.8 %multiply_convert_fusion = bf16[2,384,3072]{1,2,0:T(8,128)(2,1)S(1)} fusion(bf16[2,384,1024]{1,2,0:T(8,128)(2,1)S(1)} %copy.66, bf16[2,384,2048]{1,2,0:T(8,128)(2,1)S(1)} %copy-done.1, bf16[2,387,3072]{1,2,0:T(8,128)(2,1)S(1)} %maximum_maximum_fusion, f32[3072]{0:T(1024)S(1)} %bitcast.279, f32[3072]{0:T(1024)S(1)} %bitcast.280, f32[3072]{0:T(1024)S(1)} %bitcast.281, ...), kind=kLoop, calls=%fused_computation | loop fusion | flops 47185920 | bytes 23654400 | tf_op jit(solution)/shard_map/convert_element_type | solution.py:89
  87.4 0.2 slice.200
  87.5 0.3 slice.199
  87.8 0.0 copy-start.7
  87.9 1.0 fusion.5
  88.9 1.1 copy.70
  90.0 4.6 %all-to-all-start.1 = ((bf16[2,32,64,128]{3,2,0,1:T(8,128)(2,1)}), bf16[2,32,64,128]{3,2,0,1:T(8,128)(2,1)}, u32[]{:S(2)}, u32[]{:S(2)}) async-start(bf16[2,32,64,128]{3,2,0,1:T(8,128)(2,1)} %copy.70), calls=%async_computation.1 | async-start | bytes 2097152 | tf_op jit(solution)/shard_map/all_to_all | solution.py:154
  94.6 0.1 reshape.255
  94.7 0.9 copy.75
  95.6 0.0 copy-start.15
  95.6 25.1 %all-gather = bf16[32,3,4096]{2,1,0:T(4,128)(2,1)S(1)} all-gather(bf16[2,3,4096]{2,1,0:T(4,128)(2,1)S(1)} %copy.75), channel_id=2, replica_groups=mesh['sp'=16,'tp_0'=4,'tp_1'=2] {'sp'}, dimensions={0}, use_global_device_ids=true | all-gather | bytes 835584 | tf_op jit(solution)/shard_map/all_gather | solution.py:49
  120.7 12.7 %all-gather.1 = bf16[8,3,4096]{2,1,0:T(4,128)(2,1)S(1)} all-gather(bf16[2,3,4096]{2,1,0:T(4,128)(2,1)S(1)} %slice.201), channel_id=3, replica_groups=mesh['sp'=16,'tp_0'=4,'tp_1'=2] {'tp_0'}, dimensions={0}, use_global_device_ids=true | all-gather | bytes 245760 | tf_op jit(solution)/shard_map/all_gather | solution.py:61
  133.4 0.2 copy.76
  133.6 1.5 fusion.22
  135.1 0.0 all-to-all-done.1
  135.1 2.3 %copy.72 = bf16[8,2,4,64,128]{4,3,2,1,0:T(8,128)(2,1)} copy(bf16[8,2,4,64,128]{4,3,1,2,0:T(8,128)(2,1)} %bitcast.17) | data formatting | bytes 2097152 | tf_op jit(solution)/shard_map/all_to_all | solution.py:154
  137.5 4.9 %all-to-all-start.2 = ((bf16[16,1,4,64,128]{4,3,2,1,0:T(8,128)(2,1)}), bf16[16,1,4,64,128]{4,3,2,1,0:T(8,128)(2,1)S(1)}, u32[]{:S(2)}, u32[]{:S(2)}) async-start(bf16[16,1,4,64,128]{4,3,2,1,0:T(8,128)(2,1)} %bitcast.19), calls=%async_computation.2 | async-start | bytes 2097152 | tf_op jit(solution)/shard_map/all_to_all | solution.py:79
  142.4 2.1 %all_gather.15 = bf16[8,2,3,4096]{3,1,2,0:T(2,128)(2,1)S(1)} all-gather(bf16[4,2,3,4096]{3,1,2,0:T(2,128)(2,1)S(1)} %copy.76), channel_id=1, replica_groups=mesh['sp'=16,'tp_0'=4,'tp_1'=2] {'tp_1'}, dimensions={0}, use_global_device_ids=true | all-gather | bytes 589824 | tf_op jit(solution)/shard_map/all_gather | solution.py:61
  144.5 0.3 copy.77
  144.9 0.1 convert_reduce_fusion.1
  145.0 0.1 reshape.253
  145.1 0.1 dynamic_slice.72
  145.1 0.1 constant_dynamic-slice_fusion.4
  145.2 1.2 divide_multiply_fusion.3
  146.5 1.9 %multiply_reduce_fusion.1 = f32[]{:T(128)} fusion(bf16[1,2048]{1,0:T(2,128)(2,1)S(1)} %copy-done.4, bf16[2048,1024]{1,0:T(8,128)(2,1)} %param.16, s32[]{:T(128)S(6)} %select_n.62, f32[4,128]{1,0:T(4,128)S(1)} %get-tuple-element.9, bf16[1,3,128]{2,1,0:T(4,128)(2,1)S(1)} %get-tuple-element.5, f32[4096]{0:T(1024)S(1)} %copy-done.6, s32[]{:T(128)S(6)} %select_n.63, ...), kind=kOutput, calls=%fused_computation.113 | convolution fusion | flops 527103 | bytes 531980 | tf_op jit(solution)/shard_map/dot_general | solution.py:168
  148.3 1.5 multiply_exponential_fusion
  149.9 5.9 %all-to-all-done.2 = bf16[16,1,4,64,128]{4,3,2,1,0:T(8,128)(2,1)S(1)} async-done(((bf16[16,1,4,64,128]{4,3,2,1,0:T(8,128)(2,1)}), bf16[16,1,4,64,128]{4,3,2,1,0:T(8,128)(2,1)S(1)}, u32[]{:S(2)}, u32[]{:S(2)}) %all-to-all-start.2) | async-done | bytes 1048608 | tf_op jit(solution)/shard_map/all_to_all | solution.py:79
  155.7 0.2 convert_reduce_fusion
  155.9 0.0 copy-start.3
  155.9 0.1 fusion.56
  156.1 0.7 multiply_reduce_fusion
  157.5 0.6 fusion.45
  (44 shorter events, 0.3 us)
Async XLA Ops:
  0.6 62.9 %copy-start = (bf16[2048,256]{1,0:T(8,128)(2,1)S(1)}, bf16[2048,256]{1,0:T(8,128)(2,1)}, u32[]{:S(2)}) copy-start(bf16[2048,256]{1,0:T(8,128)(2,1)} %param.19) | copy-start | bytes 3145732
  0.6 3.0 %copy-start.10 = (f32[32]{0:T(128)S(1)}, f32[32]{0:T(128)}, u32[]{:S(2)}) copy-start(f32[32]{0:T(128)} %param.22) | copy-start | bytes 388
  4.5 61.1 %all-to-all-start = ((f32[16,2,32]{2,1,0:T(2,128)}), f32[16,2,32]{2,1,0:T(2,128)S(1)}, u32[]{:S(2)}, u32[]{:S(2)}) async-start(f32[16,2,32]{2,1,0:T(2,128)} %broadcast_in_dim.21), calls=%async_computation | async-start | bytes 32768 | tf_op jit(solution)/shard_map/all_to_all | solution.py:19
  38.6 10.2 %copy-start.14 = (f32[32]{0:T(128)S(1)}, f32[32]{0:T(128)}, u32[]{:S(2)}) copy-start(f32[32]{0:T(128)} %param.23) | copy-start | bytes 388
  41.6 10.8 %copy-start.5 = (f32[4,4096]{1,0:T(4,128)S(1)}, f32[4,4096]{1,0:T(4,128)}, u32[]{:S(2)}) copy-start(f32[4,4096]{1,0:T(4,128)} %param.20) | copy-start | bytes 196612
  43.9 22.7 %collective-permute-start = (bf16[2,3,3072]{2,0,1:T(2,128)(2,1)}, bf16[2,3,3072]{2,0,1:T(2,128)(2,1)S(1)}, u32[]{:S(2)}, u32[]{:S(2)}) collective-permute-start(bf16[2,3,3072]{2,0,1:T(2,128)(2,1)} %copy.67), channel_id=1, source_target_pairs={{0,8},{8,16},{16,24},{24,32},{32,40},{40,48},{48,56},{56,64},{64,7... | collective-permute-start | bytes 110600 | tf_op jit(solution)/shard_map/ppermute | solution.py:45
  49.5 14.1 %copy-start.4 = (bf16[1,2048]{1,0:T(2,128)(2,1)S(1)}, bf16[1,2048]{1,0:T(2,128)(2,1)}, u32[]{:S(2)}) copy-start(bf16[1,2048]{1,0:T(2,128)(2,1)} %param.14) | copy-start | bytes 12292
  52.3 12.0 %copy-start.6 = (f32[4096]{0:T(1024)S(1)}, f32[4096]{0:T(1024)}, u32[]{:S(2)}) copy-start(f32[4096]{0:T(1024)} %param.21) | copy-start | bytes 49156
  68.3 8.2 %copy-start.1 = (bf16[2,384,2048]{1,2,0:T(8,128)(2,1)S(1)}, bf16[2,384,2048]{1,2,0:T(8,128)(2,1)}, u32[]{:S(2)}) copy-start(bf16[2,384,2048]{1,2,0:T(8,128)(2,1)} %copy.65) | copy-start | bytes 9437188
  68.3 8.2 %slice-start = ((f32[4096]{0:T(1024)}), f32[3072]{0:T(1024)S(1)}, s32[]{:S(2)}) async-start(f32[4096]{0:T(1024)} %param.21), calls=%async_computation.3 | async-start | bytes 24576 | tf_op jit(solution)/shard_map/slice | solution.py:139
  87.8 6.7 %copy-start.7 = (f32[1,256]{1,0:T(1,128)S(1)}, f32[1,256]{1,0:T(1,128)}, u32[]{:S(2)}) copy-start(f32[1,256]{1,0:T(1,128)} %fusion.32) | copy-start | bytes 3076
  87.9 6.8 %copy-start.2 = (bf16[2,3,4096]{1,2,0:T(8,128)(2,1)S(1)}, bf16[2,3,4096]{1,2,0:T(8,128)(2,1)}, u32[]{:S(2)}) copy-start(bf16[2,3,4096]{1,2,0:T(8,128)(2,1)} %pad_maximum_fusion.1) | copy-start | bytes 147460
  90.0 45.1 %copy-start.8 = (f32[1,256]{1,0:T(1,128)S(1)}, f32[1,256]{1,0:T(1,128)}, u32[]{:S(2)}) copy-start(f32[1,256]{1,0:T(1,128)} %dynamic-slice.6) | copy-start | bytes 3076
  90.0 45.2 %all-to-all-start.1 = ((bf16[2,32,64,128]{3,2,0,1:T(8,128)(2,1)}), bf16[2,32,64,128]{3,2,0,1:T(8,128)(2,1)}, u32[]{:S(2)}, u32[]{:S(2)}) async-start(bf16[2,32,64,128]{3,2,0,1:T(8,128)(2,1)} %copy.70), calls=%async_computation.1 | async-start | bytes 2097152 | tf_op jit(solution)/shard_map/all_to_all | solution.py:154
  95.6 49.3 %copy-start.9 = (f32[256]{0:T(256)S(1)}, f32[256]{0:T(256)}, u32[]{:S(2)}) copy-start(f32[256]{0:T(256)} %dynamic_slice.68) | copy-start | bytes 3076
  95.6 49.5 %copy-start.15 = (f32[32]{0:T(128)S(1)}, f32[32]{0:T(128)}, u32[]{:S(2)}) copy-start(f32[32]{0:T(128)} %param.24) | copy-start | bytes 388
  133.4 14.9 %copy-start.11 = (f32[32]{0:T(128)S(1)}, f32[32]{0:T(128)}, u32[]{:S(2)}) copy-start(f32[32]{0:T(128)} %param.22) | copy-start | bytes 388
  133.4 14.9 %copy-start.13 = (f32[32]{0:T(128)S(1)}, f32[32]{0:T(128)}, u32[]{:S(2)}) copy-start(f32[32]{0:T(128)} %exponential_negate_fusion) | copy-start | bytes 388
  135.1 22.3 %copy-start.12 = (f32[4,64]{1,0:T(4,128)S(1)}, f32[4,64]{1,0:T(4,128)}, u32[]{:S(2)}) copy-start(f32[4,64]{1,0:T(4,128)} %param.25) | copy-start | bytes 3076
  137.5 18.3 %all-to-all-start.2 = ((bf16[16,1,4,64,128]{4,3,2,1,0:T(8,128)(2,1)}), bf16[16,1,4,64,128]{4,3,2,1,0:T(8,128)(2,1)S(1)}, u32[]{:S(2)}, u32[]{:S(2)}) async-start(bf16[16,1,4,64,128]{4,3,2,1,0:T(8,128)(2,1)} %bitcast.19), calls=%async_computation.2 | async-start | bytes 2097152 | tf_op jit(solution)/shard_map/all_to_all | solution.py:79
  155.9 2.1 %copy-start.3 = (bf16[4,64,128]{2,1,0:T(8,128)(2,1)}, bf16[4,64,128]{2,1,0:T(8,128)(2,1)S(1)}, u32[]{:S(2)}) copy-start(bf16[4,64,128]{2,1,0:T(8,128)(2,1)S(1)} %convert_reduce_fusion) | copy-start | bytes 196612
where the time goes:
time: 159 us; the launch traced here: 158 us
  blocking collectives  39.8 us (25%)
  other arithmetic  35.9 us (23%)
  matrix products  33.5 us (21%)
  starting transfers between devices  21.5 us (14%)
  local copies, waits for them, and re-layouts  19.6 us (12%)
  waiting for transfers between devices  5.88 us (4%)
  between operations  1.71 us (1%)
    dot_general x4, matrix products, project(): jnp.dot(flat_rows, weight, preferred_element_type=jnp.float32)  25.4 us
    all_gather x1, blocking collectives, broadcast(): lax.all_gather(value, axis)  25.1 us
    all_gather x2, blocking collectives, all_blocks(): pieces = lax.all_gather(pieces, axes[k], axis=0, tiled=True)  14.8 us
    convert_element_type x1, other arithmetic, shift_conv(): return jax.nn.silu(acc_sum).astype(jnp.bfloat16)  10.8 us
    concatenate x1, other arithmetic, per_device(): jnp.concatenate([before, joined], axis=1)  8.2 us
    all_to_all x1, starting transfers between devices, copy_for_each(): return lax.all_to_all(copies, axis, split_axis=0, concat_axis=0, tiled=True)  7.99 us
    another operation x2, other arithmetic  7.5 us
    reshape x4, local copies, waits for them, and re-layouts, project(): return result.reshape(token_rows.shape[:-1] + (weight.shape[1],))  6.86 us
  transfers between devices with their start and end apart: 4, of which 1 were waited for; matrix products, arithmetic and copies ran while one was open for 37% of the time, Pallas kernels for 0%

commit v1 on v0

--- a/solution.py
+++ b/solution.py
@@ -58,7 +58,16 @@
 def all_blocks(value, axes, sequence):
     pieces = value[None]
     for k in sequence:
-        pieces = lax.all_gather(pieces, axes[k], axis=0, tiled=True)
+        point = axes[k]
+        pieces = jnp.concatenate(
+            lax.all_to_all(
+                jnp.stack(tuple((pieces for _ in range(lax.axis_size(point))))),
+                point,
+                split_axis=0,
+                concat_axis=0,
+            ),
+            axis=0,
+        )
     held = [lax.axis_size(axes[k]) for k in reversed(sequence)]
     pieces = pieces.reshape(*held, *value.shape)
     turned = sorted(range(len(sequence)), key=lambda place: sequence[len(sequence) - 1 - place])

time: 159 us -> 174 us (1.094)
  waiting for transfers between devices: 5.88 us -> 25.9 us
  blocking collectives: 39.8 us -> 26.3 us
  starting transfers between devices: 21.5 us -> 29.5 us
    all_gather x2 -> x0, blocking collectives: 14.8 us -> none  [all_blocks(): pieces = lax.all_gather(pieces, axes[k], axis=0, tiled=True)]
    all_to_all x1, waiting for transfers between devices: 0.01 us -> 12.9 us  [per_device(): lax.all_to_all(term_full.astype(jnp.bfloat16), TP, split_axis=1, concat_a...]
    all_to_all x0 -> x2, starting transfers between devices: none -> 7.93 us  [all_blocks(): lax.all_to_all(jnp.stack(tuple((pieces for _ in range(lax.axis_size(point...]
    all_to_all x1, waiting for transfers between devices: 5.87 us -> 12.5 us  [summed_on_arrival(): lax.all_to_all(in_blocks(value, dim, devices), axis, 0, 0, tiled=True)]
    another operation x2 -> x4, local copies, waits for them, and re-layouts: 0.01 us -> 1.91 us  [the longest x2 1.9 us: all_blocks(): jnp.stack(tuple((pieces for _ in range(lax.axis_size(point)))))]
    another operation x2 -> x3, other arithmetic: 7.5 us -> 7.86 us
  transfers between devices with their start and end apart: 4 -> 6, of which waited for: 1 -> 3; matrix products, arithmetic and copies ran while one was open for 37% -> 49% of each run, Pallas kernels for 0% -> 0%
where the time goes in v1:
time: 174 us; the launch traced here: 173 us
  other arithmetic  35.5 us (20%)
  matrix products  32.9 us (19%)
  starting transfers between devices  29.5 us (17%)
  blocking collectives  26.3 us (15%)
  waiting for transfers between devices  25.9 us (15%)
  local copies, waits for them, and re-layouts  20.9 us (12%)
    all_gather x1, blocking collectives, broadcast(): lax.all_gather(value, axis)  26.3 us
    dot_general x4, matrix products, project(): jnp.dot(flat_rows, weight, preferred_element_type=jnp.float32)  25.4 us
    all_to_all x1, waiting for transfers between devices, per_device(): lax.all_to_all(term_full.astype(jnp.bfloat16), TP, split_axis=1, concat_a...  12.9 us
    all_to_all x1, waiting for transfers between devices, summed_on_arrival(): lax.all_to_all(in_blocks(value, dim, devices), axis, 0, 0, tiled=True)  12.5 us
    convert_element_type x1, other arithmetic, shift_conv(): return jax.nn.silu(acc_sum).astype(jnp.bfloat16)  10.8 us
    concatenate x1, other arithmetic, per_device(): jnp.concatenate([before, joined], axis=1)  8.2 us
    all_to_all x1, starting transfers between devices, copy_for_each(): return lax.all_to_all(copies, axis, split_axis=0, concat_axis=0, tiled=True)  7.99 us
    all_to_all x2, starting transfers between devices, all_blocks(): lax.all_to_all(jnp.stack(tuple((pieces for _ in range(lax.axis_size(point...  7.93 us
  transfers between devices with their start and end apart: 6, of which 3 were waited for; matrix products, arithmetic and copies ran while one was open for 49% of the time, Pallas kernels for 0%

profile of v1, /device:TPU:0, one launch (start us, length us, event | category | flops | bytes accessed | tf_op | source)
XLA Modules:
  0.0 172.8 jit_solution(12102890703735285609)
XLA Ops:
  0.6 0.0 copy-start
  0.6 0.0 copy-start.6
  0.7 3.0 %fusion.8 = f32[768,32]{0,1:T(8,128)S(1)} fusion(bf16[768,2048]{1,0:T(8,128)(2,1)} %bitcast.259, bf16[2048,32]{0,1:T(8,128)(2,1)} %param.18), kind=kOutput, calls=%fused_computation.16 | convolution fusion | flops 100712448 | bytes 3375104 | tf_op jit(solution)/shard_map/dot_general | solution.py:103
  3.7 0.0 copy-done.6
  3.7 0.2 fusion.77
  3.9 0.6 broadcast_in_dim.21
  4.5 8.0 %all-to-all-start = ((f32[16,2,32]{2,1,0:T(2,128)}), f32[16,2,32]{2,1,0:T(2,128)S(1)}, u32[]{:S(2)}, u32[]{:S(2)}) async-start(f32[16,2,32]{2,1,0:T(2,128)} %broadcast_in_dim.21), calls=%async_computation | async-start | bytes 32768 | tf_op jit(solution)/shard_map/all_to_all | solution.py:19
  12.5 7.7 %convolution_convert_fusion.1 = bf16[768,1024]{1,0:T(8,128)(2,1)} fusion(bf16[768,2048]{1,0:T(8,128)(2,1)} %bitcast.260, bf16[2048,1024]{1,0:T(8,128)(2,1)} %param.16), kind=kOutput, calls=%fused_computation.12 | convolution fusion | flops 3222011904 | bytes 8912896 | tf_op jit(solution)/shard_map/dot_general | solution.py:103
  20.2 1.9 %copy.65 = bf16[2,384,1024]{1,2,0:T(8,128)(2,1)S(1)} copy(bf16[2,384,1024]{2,1,0:T(8,128)(2,1)} %bitcast.266) | data formatting | bytes 3145728 | tf_op jit(solution)/shard_map/reshape | solution.py:104
  22.1 11.9 %convolution_convert_fusion = bf16[768,2048]{1,0:T(8,128)(2,1)} fusion(bf16[768,2048]{1,0:T(8,128)(2,1)} %bitcast.261, bf16[2048,2048]{1,0:T(8,128)(2,1)} %param.15), kind=kOutput, calls=%fused_computation.7 | convolution fusion | flops 6444023808 | bytes 14680064 | tf_op jit(solution)/shard_map/dot_general | solution.py:103
  34.0 4.6 %copy.64 = bf16[2,384,2048]{1,2,0:T(8,128)(2,1)} copy(bf16[2,384,2048]{2,1,0:T(8,128)(2,1)} %bitcast.264) | data formatting | bytes 6291456 | tf_op jit(solution)/shard_map/reshape | solution.py:104
  38.6 2.9 %fusion.4 = bf16[2,3,3072]{1,2,0:T(8,128)(2,1)} fusion(bf16[2,384,2048]{1,2,0:T(8,128)(2,1)} %copy.64, bf16[2,384,1024]{1,2,0:T(8,128)(2,1)S(1)} %copy.65), kind=kLoop, calls=%fused_computation.13 | loop fusion | flops 73728 | bytes 4755456 | tf_op jit(solution)/shard_map/concatenate | solution.py:143
  41.6 2.4 %copy.66 = bf16[2,3,3072]{2,0,1:T(2,128)(2,1)} copy(bf16[2,3,3072]{1,2,0:T(8,128)(2,1)} %fusion.4) | data formatting | bytes 73728 | tf_op jit(solution)/shard_map/slice | solution.py:144
  43.9 3.8 %collective-permute-start = (bf16[2,3,3072]{2,0,1:T(2,128)(2,1)}, bf16[2,3,3072]{2,0,1:T(2,128)(2,1)S(1)}, u32[]{:S(2)}, u32[]{:S(2)}) collective-permute-start(bf16[2,3,3072]{2,0,1:T(2,128)(2,1)} %copy.66), channel_id=1, source_target_pairs={{0,8},{8,16},{16,24},{24,32},{32,40},{40,48},{48,56},{56,64},{64,7... | collective-permute-start | bytes 110600 | tf_op jit(solution)/shard_map/ppermute | solution.py:45
  47.8 0.9 slice.168
  48.6 0.5 exponential_negate_fusion
  49.2 2.8 %convolution_convert_fusion.3 = bf16[6,1024]{1,0:T(8,128)(2,1)S(1)} fusion(bf16[6,2048]{1,0:T(8,128)(2,1)S(1)} %reshape.244, bf16[2048,1024]{1,0:T(8,128)(2,1)} %param.17), kind=kOutput, calls=%fused_computation.17 | convolution fusion | flops 25171968 | bytes 4231168 | tf_op jit(solution)/shard_map/dot_general | solution.py:103
  52.2 7.5 %reduce-window.6 = f32[2,32,3,128]{3,1,2,0:T(8,128)S(1)} reduce-window(f32[2,32,3,128]{3,1,2,0:T(8,128)S(1)} %bitcast.275, f32[]{:T(128)} %constant.97.clone.1), window={size=1x1x1x128 pad=0_0x0_0x0_0x0_127}, to_apply=%region_0.1 | reduce-window | flops 3121152 | bytes 196612 | tf_op jit(solution)/shard_map/reduce-window
  59.6 0.1 copy.61
  59.8 0.3 copy.73
  60.1 0.0 copy-start.5
  60.1 3.2 %pad_maximum_fusion.1 = bf16[2,3,4096]{1,2,0:T(8,128)(2,1)} fusion(bf16[2,3,1024]{1,2,0:T(8,128)(2,1)S(1)} %copy.73, bf16[2,3,3072]{1,2,0:T(8,128)(2,1)} %fusion.4), kind=kLoop, calls=%fused_computation.10 | loop fusion | flops 98304 | bytes 98304 | tf_op jit(solution)/shard_map/concatenate | solution.py:151
  63.3 2.0 %copy.74 = bf16[2,3,4096]{2,1,0:T(4,128)(2,1)S(1)} copy(bf16[2,3,4096]{1,2,0:T(8,128)(2,1)} %pad_maximum_fusion.1) | data formatting | bytes 98304 | tf_op jit(solution)/shard_map/concatenate | solution.py:151
  65.3 26.3 %all-gather = bf16[32,3,4096]{2,1,0:T(4,128)(2,1)} all-gather(bf16[2,3,4096]{2,1,0:T(4,128)(2,1)S(1)} %copy.74), channel_id=2, replica_groups=mesh['sp'=16,'tp_0'=4,'tp_1'=2] {'sp'}, dimensions={0}, use_global_device_ids=true | all-gather | bytes 835584 | tf_op jit(solution)/shard_map/all_gather | solution.py:49
  91.6 0.2 fusion.32
  91.8 0.0 copy-done.5
  91.8 0.1 dynamic_slice.71
  91.9 0.1 dynamic-slice.6
  92.0 0.9 slice.201
  92.9 0.1 copy.75
  92.9 0.8 stack.6
  93.8 4.5 %all-to-all-start.3 = ((bf16[4,1,2,3,4096]{4,2,3,1,0:T(2,128)(2,1)}), bf16[4,1,2,3,4096]{4,2,3,1,0:T(2,128)(2,1)S(1)}, u32[]{:S(2)}, u32[]{:S(2)}) async-start(bf16[4,1,2,3,4096]{4,2,3,1,0:T(2,128)(2,1)} %stack.6), calls=%async_computation.3 | async-start | bytes 393216 | tf_op jit(solution)/shard_map/all_to_all | solution.py:63
  98.2 0.1 broadcast_select_fusion
  98.4 0.2 fusion.30
  98.6 1.6 copy.67
  100.2 8.2 %maximum_maximum_fusion = bf16[2,387,3072]{1,2,0:T(8,128)(2,1)S(1)} fusion(bf16[2,384,1024]{1,2,0:T(8,128)(2,1)S(1)} %copy.65, bf16[2,384,2048]{1,2,0:T(8,128)(2,1)} %copy.64, bf16[2,3,3072]{1,2,0:T(8,128)(2,1)} %copy.67), kind=kLoop, calls=%fused_computation.1 | loop fusion | flops 14266368 | bytes 9510912 | tf_op jit(solution)/shard_map/concatenate | solution.py:146
  108.5 10.8 %multiply_convert_fusion = bf16[2,384,3072]{1,2,0:T(8,128)(2,1)S(1)} fusion(bf16[2,384,1024]{1,2,0:T(8,128)(2,1)S(1)} %copy.65, bf16[2,384,2048]{1,2,0:T(8,128)(2,1)S(1)} %copy-done.1, bf16[2,387,3072]{1,2,0:T(8,128)(2,1)S(1)} %maximum_maximum_fusion, f32[3072]{0:T(1024)S(1)} %bitcast.278, f32[3072]{0:T(1024)S(1)} %bitcast.279, f32[3072]{0:T(1024)S(1)} %bitcast.280, ...), kind=kLoop, calls=%fused_computation | loop fusion | flops 47185920 | bytes 23654400 | tf_op jit(solution)/shard_map/convert_element_type | solution.py:98
  119.3 0.2 slice.200
  119.5 0.3 slice.199
  119.8 1.0 fusion.5
  120.8 1.1 copy.69
  121.9 4.8 %all-to-all-start.1 = ((bf16[2,32,64,128]{3,2,0,1:T(8,128)(2,1)}), bf16[2,32,64,128]{3,2,0,1:T(8,128)(2,1)S(1)}, u32[]{:S(2)}, u32[]{:S(2)}) async-start(bf16[2,32,64,128]{3,2,0,1:T(8,128)(2,1)} %copy.69), calls=%async_computation.1 | async-start | bytes 2097152 | tf_op jit(solution)/shard_map/all_to_all | solution.py:163
  126.7 0.1 reshape.255
  126.8 0.1 dynamic_slice.75
  126.9 1.5 fusion.22
  128.3 0.4 pad_maximum_fusion.2
  128.7 1.1 copy.76
  129.8 12.9 %all-to-all-done.1 = bf16[2,32,64,128]{3,2,0,1:T(8,128)(2,1)S(1)} async-done(((bf16[2,32,64,128]{3,2,0,1:T(8,128)(2,1)}), bf16[2,32,64,128]{3,2,0,1:T(8,128)(2,1)S(1)}, u32[]{:S(2)}, u32[]{:S(2)}) %all-to-all-start.1) | async-done | bytes 1048608 | tf_op jit(solution)/shard_map/all_to_all | solution.py:163
  142.6 3.5 %all-to-all-start.4 = ((bf16[2,4,2,3,4096]{4,1,3,2,0:T(4,128)(2,1)}), bf16[2,4,2,3,4096]{4,1,3,2,0:T(4,128)(2,1)S(1)}, u32[]{:S(2)}, u32[]{:S(2)}) async-start(bf16[2,4,2,3,4096]{4,1,3,2,0:T(4,128)(2,1)} %copy.76), calls=%async_computation.4 | async-start | bytes 786432 | tf_op jit(solution)/shard_map/all_to_all | solution.py:63
  146.1 1.1 copy.71
  147.2 0.6 all-to-all-done.4
  147.7 5.0 %all-to-all-start.2 = ((bf16[16,1,4,64,128]{4,3,2,1,0:T(8,128)(2,1)}), bf16[16,1,4,64,128]{4,3,2,1,0:T(8,128)(2,1)S(1)}, u32[]{:S(2)}, u32[]{:S(2)}) async-start(bf16[16,1,4,64,128]{4,3,2,1,0:T(8,128)(2,1)} %bitcast.19), calls=%async_computation.2 | async-start | bytes 2097152 | tf_op jit(solution)/shard_map/all_to_all | solution.py:88
  152.7 0.3 copy.77
  153.1 0.1 convert_reduce_fusion.1
  153.2 0.1 reshape.253
  153.3 0.1 constant_dynamic-slice_fusion.4
  153.3 1.2 divide_multiply_fusion.3
  154.6 1.9 %multiply_reduce_fusion.1 = f32[]{:T(128)} fusion(bf16[1,2048]{1,0:T(2,128)(2,1)S(1)} %copy-done.3, bf16[2048,1024]{1,0:T(8,128)(2,1)} %param.16, s32[]{:T(128)S(6)} %select_n.62, f32[4,128]{1,0:T(4,128)S(1)} %get-tuple-element.9, bf16[1,3,128]{2,1,0:T(4,128)(2,1)S(1)} %get-tuple-element.5, f32[4096]{0:T(1024)S(1)} %copy-done.5, s32[]{:T(128)S(6)} %select_n.63, ...), kind=kOutput, calls=%fused_computation.114 | convolution fusion | flops 527103 | bytes 531980 | tf_op jit(solution)/shard_map/dot_general | solution.py:177
  156.4 1.5 multiply_exponential_fusion
  158.0 12.5 %all-to-all-done.2 = bf16[16,1,4,64,128]{4,3,2,1,0:T(8,128)(2,1)S(1)} async-done(((bf16[16,1,4,64,128]{4,3,2,1,0:T(8,128)(2,1)}), bf16[16,1,4,64,128]{4,3,2,1,0:T(8,128)(2,1)S(1)}, u32[]{:S(2)}, u32[]{:S(2)}) %all-to-all-start.2) | async-done | bytes 1048608 | tf_op jit(solution)/shard_map/all_to_all | solution.py:88
  170.5 0.2 convert_reduce_fusion
  170.7 0.1 fusion.56
  170.8 0.7 multiply_reduce_fusion
  172.2 0.6 fusion.45
  (41 shorter events, 0.2 us)
Async XLA Ops:
  0.6 90.9 %copy-start = (bf16[2048,256]{1,0:T(8,128)(2,1)S(1)}, bf16[2048,256]{1,0:T(8,128)(2,1)}, u32[]{:S(2)}) copy-start(bf16[2048,256]{1,0:T(8,128)(2,1)} %param.19) | copy-start | bytes 3145732
  0.6 3.0 %copy-start.6 = (f32[32]{0:T(128)S(1)}, f32[32]{0:T(128)}, u32[]{:S(2)}) copy-start(f32[32]{0:T(128)} %param.22) | copy-start | bytes 388
  4.5 88.4 %all-to-all-start = ((f32[16,2,32]{2,1,0:T(2,128)}), f32[16,2,32]{2,1,0:T(2,128)S(1)}, u32[]{:S(2)}, u32[]{:S(2)}) async-start(f32[16,2,32]{2,1,0:T(2,128)} %broadcast_in_dim.21), calls=%async_computation | async-start | bytes 32768 | tf_op jit(solution)/shard_map/all_to_all | solution.py:19
  38.6 10.0 %copy-start.10 = (f32[32]{0:T(128)S(1)}, f32[32]{0:T(128)}, u32[]{:S(2)}) copy-start(f32[32]{0:T(128)} %param.23) | copy-start | bytes 388
  41.6 10.5 %copy-start.4 = (f32[4,4096]{1,0:T(4,128)S(1)}, f32[4,4096]{1,0:T(4,128)}, u32[]{:S(2)}) copy-start(f32[4,4096]{1,0:T(4,128)} %param.20) | copy-start | bytes 196612
  43.9 54.7 %collective-permute-start = (bf16[2,3,3072]{2,0,1:T(2,128)(2,1)}, bf16[2,3,3072]{2,0,1:T(2,128)(2,1)S(1)}, u32[]{:S(2)}, u32[]{:S(2)}) collective-permute-start(bf16[2,3,3072]{2,0,1:T(2,128)(2,1)} %copy.66), channel_id=1, source_target_pairs={{0,8},{8,16},{16,24},{24,32},{32,40},{40,48},{48,56},{56,64},{64,7... | collective-permute-start | bytes 110600 | tf_op jit(solution)/shard_map/ppermute | solution.py:45
  52.1 39.4 %copy-start.3 = (bf16[1,2048]{1,0:T(2,128)(2,1)S(1)}, bf16[1,2048]{1,0:T(2,128)(2,1)}, u32[]{:S(2)}) copy-start(bf16[1,2048]{1,0:T(2,128)(2,1)} %param.14) | copy-start | bytes 12292
  60.1 31.7 %copy-start.5 = (f32[4096]{0:T(1024)S(1)}, f32[4096]{0:T(1024)}, u32[]{:S(2)}) copy-start(f32[4096]{0:T(1024)} %param.21) | copy-start | bytes 49156
  63.3 35.1 %copy-start.7 = (f32[32]{0:T(128)S(1)}, f32[32]{0:T(128)}, u32[]{:S(2)}) copy-start(f32[32]{0:T(128)} %param.22) | copy-start | bytes 388
  63.3 35.1 %copy-start.9 = (f32[32]{0:T(128)S(1)}, f32[32]{0:T(128)}, u32[]{:S(2)}) copy-start(f32[32]{0:T(128)} %exponential_negate_fusion) | copy-start | bytes 388
  93.8 28.1 %all-to-all-start.3 = ((bf16[4,1,2,3,4096]{4,2,3,1,0:T(2,128)(2,1)}), bf16[4,1,2,3,4096]{4,2,3,1,0:T(2,128)(2,1)S(1)}, u32[]{:S(2)}, u32[]{:S(2)}) async-start(bf16[4,1,2,3,4096]{4,2,3,1,0:T(2,128)(2,1)} %stack.6), calls=%async_computation.3 | async-start | bytes 393216 | tf_op jit(solution)/shard_map/all_to_all | solution.py:63
  100.2 8.2 %copy-start.1 = (bf16[2,384,2048]{1,2,0:T(8,128)(2,1)S(1)}, bf16[2,384,2048]{1,2,0:T(8,128)(2,1)}, u32[]{:S(2)}) copy-start(bf16[2,384,2048]{1,2,0:T(8,128)(2,1)} %copy.64) | copy-start | bytes 9437188
  100.2 8.2 %slice-start = ((f32[4096]{0:T(1024)}), f32[3072]{0:T(1024)S(1)}, s32[]{:S(2)}) async-start(f32[4096]{0:T(1024)} %param.21), calls=%async_computation.5 | async-start | bytes 24576 | tf_op jit(solution)/shard_map/slice | solution.py:148
  119.8 7.0 %copy-start.11 = (f32[32]{0:T(128)S(1)}, f32[32]{0:T(128)}, u32[]{:S(2)}) copy-start(f32[32]{0:T(128)} %param.24) | copy-start | bytes 388
  121.9 20.7 %all-to-all-start.1 = ((bf16[2,32,64,128]{3,2,0,1:T(8,128)(2,1)}), bf16[2,32,64,128]{3,2,0,1:T(8,128)(2,1)S(1)}, u32[]{:S(2)}, u32[]{:S(2)}) async-start(bf16[2,32,64,128]{3,2,0,1:T(8,128)(2,1)} %copy.69), calls=%async_computation.1 | async-start | bytes 2097152 | tf_op jit(solution)/shard_map/all_to_all | solution.py:163
  129.8 42.4 %copy-start.8 = (f32[4,64]{1,0:T(4,128)S(1)}, f32[4,64]{1,0:T(4,128)}, u32[]{:S(2)}) copy-start(f32[4,64]{1,0:T(4,128)} %param.25) | copy-start | bytes 3076
  142.6 5.1 %all-to-all-start.4 = ((bf16[2,4,2,3,4096]{4,1,3,2,0:T(4,128)(2,1)}), bf16[2,4,2,3,4096]{4,1,3,2,0:T(4,128)(2,1)S(1)}, u32[]{:S(2)}, u32[]{:S(2)}) async-start(bf16[2,4,2,3,4096]{4,1,3,2,0:T(4,128)(2,1)} %copy.76), calls=%async_computation.4 | async-start | bytes 786432 | tf_op jit(solution)/shard_map/all_to_all | solution.py:63
  147.7 22.8 %all-to-all-start.2 = ((bf16[16,1,4,64,128]{4,3,2,1,0:T(8,128)(2,1)}), bf16[16,1,4,64,128]{4,3,2,1,0:T(8,128)(2,1)S(1)}, u32[]{:S(2)}, u32[]{:S(2)}) async-start(bf16[16,1,4,64,128]{4,3,2,1,0:T(8,128)(2,1)} %bitcast.19), calls=%async_computation.2 | async-start | bytes 2097152 | tf_op jit(solution)/shard_map/all_to_all | solution.py:88
  170.7 2.1 %copy-start.2 = (bf16[4,64,128]{2,1,0:T(8,128)(2,1)}, bf16[4,64,128]{2,1,0:T(8,128)(2,1)S(1)}, u32[]{:S(2)}) copy-start(bf16[4,64,128]{2,1,0:T(8,128)(2,1)S(1)} %convert_reduce_fusion) | copy-start | bytes 196612
